TPU v7x, 32 devices: a whole 2x2x4 slice. The times are simulated.
32 devices in a mesh: rep: 2 (over x), fs: 8 (over z, y), tp: 2 (over core).
Axes of the slice: x: 2, y: 2, z: 4, core: 2. Of those that a mesh axis runs over, the one named last changes fastest.
Arguments:
- inputs: bfloat16 [8192, 1024], P(('rep', 'fs', 'tp')), may hold values from -6 to 6
- up_proj: bfloat16 [1024, 4096], P('fs', 'tp'), may hold values from -0.1875 to 0.1875
- down_proj: bfloat16 [4096, 1024], P('tp', 'fs'), may hold values from -0.09375 to 0.09375
- out_cotangent: bfloat16 [8192, 1024], P(('rep', 'fs', 'tp')), may hold values from -6 to 6
Outputs:
- grad_inputs: bfloat16 [8192, 1024], P(('rep', 'fs', 'tp'))
- grad_up: float32 [1024, 4096], P('fs', 'tp')
- grad_down: float32 [4096, 1024], P('tp', 'fs')
- energy_up: float32 [1024], P('fs')
- energy_down: float32 [4096], P('tp')
All inputs are finite; a program needn't handle non-finite values.
Results may differ from a plain program's by a relative error of at most 0.001.
Values may be sent and summed in bfloat16 or wider, within the bound.
A program may use at most 128 MiB of HBM per device.

v0:
```python
import jax
import jax.numpy as jnp
from jax import lax
from jax.sharding import PartitionSpec as P

D = 1024
FF = 4096


def taken_in(shard, axis, dim, absorb, state):
    everything = jax.tree.map(lambda a: lax.all_gather(a, axis, axis=dim, tiled=True), shard)
    return absorb(state, everything, jnp.int32(0))


def summed_rows(product, span, axis):
    whole = product(jnp.int32(0), span * lax.axis_size(axis))
    return lax.psum_scatter(whole, axis, scatter_dimension=0, tiled=True)


def contract(left, right, left_dim, right_dim):
    return lax.dot_general(
        left, right, (((left_dim,), (right_dim,)), ((), ())), preferred_element_type=jnp.float32
    )


def body(inputs, up_proj, down_proj, out_cotangent):
    factor = float(
        inputs.shape[0] * lax.axis_size("rep") * lax.axis_size("fs") * lax.axis_size("tp")
    ) ** (-0.5)
    all_inputs, all_cotangent = (
        lax.all_gather(inputs, "tp", axis=0, tiled=True),
        lax.all_gather(out_cotangent, "tp", axis=0, tiled=True),
    )
    hidden_cols = up_proj.shape[1]
    group_rows = all_inputs.shape[0]
    whole_up = lax.all_gather(up_proj, "fs", axis=0, tiled=True)
    pre = jnp.dot(all_inputs, whole_up, preferred_element_type=jnp.float32)
    active = jnp.square(jax.nn.relu(pre)).astype(jnp.bfloat16)

    def add_cols(total, piece, start):
        columns = lax.dynamic_slice_in_dim(all_cotangent, start, piece.shape[1], 1)
        return total + contract(columns, piece, 1, 1)

    back = taken_in(down_proj, "fs", 1, add_cols, jnp.zeros((group_rows, hidden_cols), jnp.float32))
    grad_pre = (2.0 * jax.nn.relu(pre) * back).astype(jnp.bfloat16)

    def input_part(start, count):
        rows = lax.dynamic_slice_in_dim(grad_pre, start, count, 0)
        return contract(rows, whole_up, 1, 1)

    grad_inputs = summed_rows(input_part, inputs.shape[0], "tp")
    grad_inputs = grad_inputs.astype(jnp.bfloat16)
    shard_rows = up_proj.shape[0]

    def up_part(start, count):
        columns = lax.dynamic_slice_in_dim(all_inputs, start, count, 1)
        return contract(columns, grad_pre, 0, 0) * factor

    def down_part(start, count):
        columns = lax.dynamic_slice_in_dim(all_cotangent, start, count, 1)
        return contract(columns, active, 0, 0) * factor

    def joint_part(start, count):
        return jnp.concatenate([up_part(start, count), down_part(start, count)], axis=1)

    joint_local = summed_rows(joint_part, shard_rows, "fs")
    joint_sum = lax.psum(joint_local, "rep")
    grad_up = joint_sum[:, :hidden_cols]
    down_flip = joint_sum[:, hidden_cols:]
    grad_down = jnp.transpose(down_flip)
    energy_up = lax.psum(jnp.sum(grad_up * grad_up, axis=1), "tp") / FF
    energy_down = lax.psum(jnp.sum(grad_down * grad_down, axis=1), "fs") / D
    return (grad_inputs, grad_up, grad_down, energy_up, energy_down)


def solution(mesh):
    return jax.shard_map(
        body,
        mesh=mesh,
        in_specs=(
            P(("rep", "fs", "tp"), None),
            P("fs", "tp"),
            P("tp", "fs"),
            P(("rep", "fs", "tp"), None),
        ),
        out_specs=(P(("rep", "fs", "tp"), None), P("fs", "tp"), P("tp", "fs"), P("fs"), P("tp")),
        check_vma=False,
    )
```

profile of v0, /device:TPU:0, one launch (start us, length us, event | category | flops | bytes accessed | tf_op | source)
XLA Modules:
  0.0 594.2 jit_solution(6875754057752719887)
XLA Ops:
  7.2 0.0 all-gather.5.cloned.1.call-start
  7.2 0.7 all-gather.5.cloned.1.call-update
  7.9 0.0 all-gather.7.cloned.1.call-start
  7.9 0.7 all-gather.7.cloned.1.call-update
  8.6 0.0 all-gather.9.cloned.1.call-start
  8.7 0.7 all-gather.9.cloned.1.call-update
  9.4 0.0 all-gather.11.cloned.1.call-start
  9.4 0.5 all-gather.11.cloned.1.call-update
  10.0 0.0 reduce-scatter.5.cloned.1.call-start
  10.0 11.3 %all-gather.5.cloned.1.call-done = bf16[512,1024]{1,0:T(8,128)(2,1)} async-done(((bf16[256,1024]{1,0:T(8,128)(2,1)}), bf16[512,1024]{1,0:T(8,128)(2,1)}) %all-gather.5.cloned.1.call-update) | async-done | bytes 1048592 | tf_op jit(solution)/shard_map/all_gather | solution.py:31
  21.3 76.1 %all-gather.7.cloned.1.call-done = bf16[1024,2048]{1,0:T(8,128)(2,1)} async-done(((bf16[128,2048]{1,0:T(8,128)(2,1)}), bf16[1024,2048]{1,0:T(8,128)(2,1)}) %all-gather.7.cloned.1.call-update) | async-done | bytes 4194320 | tf_op jit(solution)/shard_map/all_gather | solution.py:36
  97.4 6.8 %fusion.2 = f32[512,2048]{1,0:T(8,128)} fusion(bf16[512,1024]{1,0:T(8,128)(2,1)} %all-gather.5.cloned.1.call-done, bf16[1024,2048]{1,0:T(8,128)(2,1)} %all-gather.7.cloned.1.call-done), kind=kOutput, calls=%fused_computation.12 | convolution fusion | flops 2147483648 | bytes 9437184 | tf_op jit(solution)/shard_map/dot_general | solution.py:37
  104.2 2.4 all-gather.9.cloned.1.call-done
  106.6 0.0 copy-start.1
  106.6 8.2 %multiply_bitcast_fusion = f32[1024,2048]{0,1:T(8,128)} fusion(bf16[512,1024]{1,0:T(8,128)(2,1)} %all-gather.9.cloned.1.call-done, f32[512,2048]{1,0:T(8,128)} %fusion.2), kind=kOutput, calls=%fused_computation.1 | convolution fusion | flops 2152726528 | bytes 13631488 | tf_op jit(solution)/shard_map/dot_general | solution.py:21
  114.8 0.0 copy-start.2
  114.8 69.5 %all-gather.11.cloned.1.call-done = bf16[2048,1024]{1,0:T(8,128)(2,1)} async-done(((bf16[2048,128]{1,0:T(8,128)(2,1)}), bf16[2048,1024]{1,0:T(8,128)(2,1)}) %all-gather.11.cloned.1.call-update) | async-done | bytes 4194320 | tf_op jit(solution)/shard_map/all_gather | solution.py:11
  184.3 0.0 copy-done.1
  184.3 5.9 multiply_convert_fusion.1
  190.2 0.0 copy-done.2
  190.2 0.0 copy-start.3
  190.2 0.0 copy-start
  190.2 2.4 multiply_bitcast_fusion.1
  192.6 0.0 copy-done.3
  192.6 1.7 copy-done
  194.3 6.4 %pad_maximum_fusion = f32[1024,4096]{0,1:T(8,128)} fusion(f32[1024,2048]{0,1:T(8,128)S(1)} %copy-done, f32[1024,2048]{0,1:T(8,128)S(1)} %multiply_bitcast_fusion.1), kind=kLoop, calls=%fused_computation | loop fusion | flops 4194304 | bytes 33554432 | tf_op jit(solution)/shard_map/concatenate | solution.py:64
  200.7 0.0 copy-start.4
  200.7 0.0 reduce-scatter.5.cloned.1.call-update
  200.8 0.0 reduce-scatter.3.cloned.1.call-start
  200.8 1.5 copy-done.4
  202.3 5.9 fusion.3
  208.2 0.0 reduce-scatter.3.cloned.1.call-update
  208.3 0.0 all-reduce.2.cloned.1.call-start
  208.3 271.0 %reduce-scatter.5.cloned.1.call-done = f32[128,4096]{0,1:T(8,128)} async-done(((f32[1024,4096]{0,1:T(8,128)}), f32[128,4096]{0,1:T(8,128)}) %reduce-scatter.5.cloned.1.call-update) | async-done | bytes 2097168 | tf_op jit(solution)/shard_map/reduce_scatter | solution.py:17
  479.3 0.0 all-reduce.2.cloned.1.call-update
  479.4 11.0 %reduce-scatter.3.cloned.1.call-done = f32[256,1024]{1,0:T(8,128)} async-done(((f32[512,1024]{1,0:T(8,128)}), f32[256,1024]{1,0:T(8,128)}) %reduce-scatter.3.cloned.1.call-update) | async-done | bytes 1048592 | tf_op jit(solution)/shard_map/reduce_scatter | solution.py:17
  490.3 2.1 convert_element_type.10
  492.4 64.5 %all-reduce.2.cloned.1.call-done = f32[128,4096]{0,1:T(8,128)} async-done(((f32[128,4096]{0,1:T(8,128)}), f32[128,4096]{0,1:T(8,128)}) %all-reduce.2.cloned.1.call-update) | async-done | bytes 2097168 | tf_op jit(solution)/shard_map/psum | solution.py:67
  556.9 2.4 multiply_reduce_fusion
  559.3 21.7 %psum.23 = f32[2048]{0:T(1024)S(1)} all-reduce(f32[2048]{0:T(1024)S(1)} %get-tuple-element.10), channel_id=1, replica_groups=mesh['rep'=2,'fs'=8,'tp'=2] {'fs'}, use_global_device_ids=true, to_apply=%region_6.7 | all-reduce | flops 2048 | bytes 16384 | tf_op jit(solution)/shard_map/psum | solution.py:72
  581.0 0.6 broadcast_multiply_fusion
  581.6 1.5 multiply_reduce_fusion.1
  583.1 2.5 psum.22
  585.6 0.5 broadcast_multiply_fusion.1
  586.1 1.3 copy.9
Async XLA Ops:
  7.2 14.1 %all-gather.5.cloned.1.call-start = ((), (), s32[]{:S(2)}) async-start(), calls=%async_computation.2 | async-start | bytes 1572864 | tf_op jit(solution)/shard_map/all_gather | solution.py:31
  7.9 89.5 %all-gather.7.cloned.1.call-start = ((), (), s32[]{:S(2)}) async-start(), calls=%async_computation.3 | async-start | bytes 4718592 | tf_op jit(solution)/shard_map/all_gather | solution.py:36
  8.6 97.9 %all-gather.9.cloned.1.call-start = ((), (), s32[]{:S(2)}) async-start(), calls=%async_computation.4 | async-start | bytes 1572864 | tf_op jit(solution)/shard_map/all_gather | solution.py:32
  9.4 174.9 %all-gather.11.cloned.1.call-start = ((), (), s32[]{:S(2)}) async-start(), calls=%async_computation.5 | async-start | bytes 4718592 | tf_op jit(solution)/shard_map/all_gather | solution.py:11
  10.0 469.4 %reduce-scatter.5.cloned.1.call-start = ((), (), s32[]{:S(2)}) async-start(), calls=%async_computation.7 | async-start | bytes 18874368 | tf_op jit(solution)/shard_map/reduce_scatter | solution.py:17
  106.6 77.7 %copy-start.1 = (bf16[512,1024]{1,0:T(8,128)(2,1)S(1)}, bf16[512,1024]{1,0:T(8,128)(2,1)}, u32[]{:S(2)}) copy-start(bf16[512,1024]{1,0:T(8,128)(2,1)} %all-gather.9.cloned.1.call-done) | copy-start | bytes 3145732
  114.8 75.4 %copy-start.2 = (bf16[512,1024]{1,0:T(8,128)(2,1)S(1)}, bf16[512,1024]{1,0:T(8,128)(2,1)}, u32[]{:S(2)}) copy-start(bf16[512,1024]{1,0:T(8,128)(2,1)} %all-gather.5.cloned.1.call-done) | copy-start | bytes 3145732
  190.2 2.4 copy-start.3
  190.2 4.1 copy-start
  200.7 1.6 copy-start.4
  200.8 289.6 %reduce-scatter.3.cloned.1.call-start = ((), (), s32[]{:S(2)}) async-start(), calls=%async_computation.6 | async-start | bytes 3145728 | tf_op jit(solution)/shard_map/reduce_scatter | solution.py:17
  208.3 348.7 %all-reduce.2.cloned.1.call-start = ((), (), s32[]{:S(2)}) async-start(), calls=%async_computation.8 | async-start | bytes 4194304 | tf_op jit(solution)/shard_map/psum | solution.py:67
Sparse Core Ops, SparseCore 0:
  9.5 11.7 all-gather.4
  23.4 73.9 all-gather.6
  99.0 7.5 all-gather.8
  108.5 75.7 all-gather.10
  200.9 278.4 reduce-scatter.4
  481.4 8.8 reduce-scatter.2
  492.6 64.2 all-reduce.1
where the time goes:
time: 595 us; the launch traced here: 594 us
  waiting for transfers between devices  508 us (85%)
  matrix products  29.2 us (5%)
  blocking collectives  24.1 us (4%)
  between operations  14.2 us (2%)
  other arithmetic  13.5 us (2%)
    reduce_scatter x2, waiting for transfers between devices, summed_rows(): return lax.psum_scatter(whole, axis, scatter_dimension=0, tiled=True)  282 us
    all_gather x1, waiting for transfers between devices, body(): whole_up = lax.all_gather(up_proj, 'fs', axis=0, tiled=True)  76.1 us
    all_gather x1, waiting for transfers between devices, taken_in(): lax.all_gather(a, axis, axis=dim, tiled=True)  69.5 us
    psum x1, waiting for transfers between devices, body(): joint_sum = lax.psum(joint_local, 'rep')  64.5 us
    dot_general x4, matrix products, contract(): lax.dot_general(left, right, (((left_dim,), (right_dim,)), ((), ())), pre...  22.4 us
    psum x1, blocking collectives, body(): energy_down = lax.psum(jnp.sum(grad_down * grad_down, axis=1), 'fs') / D  21.7 us
  transfers between devices with their start and end apart: 7, of which 7 were waited for; matrix products, arithmetic and copies ran while one was open for 4% of the time, Pallas kernels for 0%

commit v1 on v0

--- a/solution.py
+++ b/solution.py
@@ -5,6 +5,17 @@
 
 D = 1024
 FF = 4096
+
+
+def gather_around(shard, axis, dim):
+    ways = lax.axis_size(axis)
+    pieces = [shard]
+    for far in range(1, ways):
+        pieces.append(
+            lax.ppermute(pieces[far - 1], axis, [(d, (d - 1) % ways) for d in range(ways)])
+        )
+    line = jnp.concatenate(pieces, axis=dim)
+    return jnp.roll(line, lax.axis_index(axis) * shard.shape[dim], axis=dim)
 
 
 def taken_in(shard, axis, dim, absorb, state):
@@ -33,7 +44,7 @@
     )
     hidden_cols = up_proj.shape[1]
     group_rows = all_inputs.shape[0]
-    whole_up = lax.all_gather(up_proj, "fs", axis=0, tiled=True)
+    whole_up = gather_around(up_proj, "fs", 0)
     pre = jnp.dot(all_inputs, whole_up, preferred_element_type=jnp.float32)
     active = jnp.square(jax.nn.relu(pre)).astype(jnp.bfloat16)
 

time: 595 us -> 594 us (level)
  waiting for transfers between devices: 508 us -> 455 us
  starting transfers between devices: 0.27 us -> 37.5 us
  local copies, waits for them, and re-layouts: 4.54 us -> 19.5 us
    ppermute x0 -> x7, waiting for transfers between devices: none -> 103 us  [gather_around(): lax.ppermute(pieces[far - 1], axis, [(d, (d - 1) % ways) for d in range(w...]
    all_gather x1 -> x0, waiting for transfers between devices: 76.1 us -> none  [body(): whole_up = lax.all_gather(up_proj, 'fs', axis=0, tiled=True)]
    all_gather x1, waiting for transfers between devices: 69.5 us -> 0.01 us  [taken_in(): lax.all_gather(a, axis, axis=dim, tiled=True)]
    ppermute x0 -> x7, starting transfers between devices: none -> 37.1 us  [gather_around(): lax.ppermute(pieces[far - 1], axis, [(d, (d - 1) % ways) for d in range(w...]
    unnamed x11 -> x28, local copies, waits for them, and re-layouts: 4.54 us -> 18.6 us
    all_gather x1, waiting for transfers between devices: 11.3 us -> 0.01 us  [body(): lax.all_gather(inputs, 'tp', axis=0, tiled=True)]
  transfers between devices with their start and end apart: 7 -> 13, of which waited for: 7 -> 10; matrix products, arithmetic and copies ran while one was open for 4% -> 6% of each run, Pallas kernels for 0% -> 0%
where the time goes in v1:
time: 594 us; the launch traced here: 593 us
  waiting for transfers between devices  455 us (77%)
  starting transfers between devices  37.5 us (6%)
  matrix products  29.2 us (5%)
  blocking collectives  24.1 us (4%)
  local copies, waits for them, and re-layouts  19.5 us (3%)
  between operations  14.2 us (2%)
  other arithmetic  13.5 us (2%)
    reduce_scatter x2, waiting for transfers between devices, summed_rows(): return lax.psum_scatter(whole, axis, scatter_dimension=0, tiled=True)  286 us
    ppermute x7, waiting for transfers between devices, gather_around(): lax.ppermute(pieces[far - 1], axis, [(d, (d - 1) % ways) for d in range(w...  103 us
    psum x1, waiting for transfers between devices, body(): joint_sum = lax.psum(joint_local, 'rep')  64.3 us
    ppermute x7, starting transfers between devices, gather_around(): lax.ppermute(pieces[far - 1], axis, [(d, (d - 1) % ways) for d in range(w...  37.1 us
    dot_general x4, matrix products, contract(): lax.dot_general(left, right, (((left_dim,), (right_dim,)), ((), ())), pre...  22.4 us
    psum x1, blocking collectives, body(): energy_down = lax.psum(jnp.sum(grad_down * grad_down, axis=1), 'fs') / D  21.7 us
    unnamed x28, local copies, waits for them, and re-layouts  18.6 us
  transfers between devices with their start and end apart: 13, of which 10 were waited for; matrix products, arithmetic and copies ran while one was open for 6% of the time, Pallas kernels for 0%

profile of v1, /device:TPU:0, one launch (start us, length us, event | category | flops | bytes accessed | tf_op | source)
XLA Modules:
  0.0 593.1 jit_solution(229082176077833551)
XLA Ops:
  9.4 6.1 %collective-permute-start = (bf16[128,2048]{1,0:T(8,128)(2,1)}, bf16[128,2048]{1,0:T(8,128)(2,1)S(1)}, u32[]{:S(2)}, u32[]{:S(2)}) collective-permute-start(bf16[128,2048]{1,0:T(8,128)(2,1)} %param.5), channel_id=1, source_target_pairs={{0,14},{2,0},{4,2},{6,4},{8,6},{10,8},{12,10},{14,12},{1,15},{3,1}... | collective-permute-start | bytes 1572872 | tf_op jit(solution)/shard_map/ppermute | solution.py:15
  15.5 11.5 %collective-permute-done = bf16[128,2048]{1,0:T(8,128)(2,1)S(1)} collective-permute-done((bf16[128,2048]{1,0:T(8,128)(2,1)}, bf16[128,2048]{1,0:T(8,128)(2,1)S(1)}, u32[]{:S(2)}, u32[]{:S(2)}) %collective-permute-start) | collective-permute-done | bytes 524320 | tf_op jit(solution)/shard_map/ppermute | solution.py:15
  27.0 5.1 collective-permute-start.1
  32.1 10.3 %collective-permute-done.1 = bf16[128,2048]{1,0:T(8,128)(2,1)S(1)} collective-permute-done((bf16[128,2048]{1,0:T(8,128)(2,1)S(1)}, bf16[128,2048]{1,0:T(8,128)(2,1)S(1)}, u32[]{:S(2)}, u32[]{:S(2)}) %collective-permute-start.1) | collective-permute-done | bytes 524320 | tf_op jit(solution)/shard_map/ppermute | solution.py:15
  42.4 5.2 collective-permute-start.2
  47.6 19.0 %collective-permute-done.2 = bf16[128,2048]{1,0:T(8,128)(2,1)S(1)} collective-permute-done((bf16[128,2048]{1,0:T(8,128)(2,1)S(1)}, bf16[128,2048]{1,0:T(8,128)(2,1)S(1)}, u32[]{:S(2)}, u32[]{:S(2)}) %collective-permute-start.2) | collective-permute-done | bytes 524320 | tf_op jit(solution)/shard_map/ppermute | solution.py:15
  66.6 5.2 collective-permute-start.3
  71.8 12.8 %collective-permute-done.3 = bf16[128,2048]{1,0:T(8,128)(2,1)S(1)} collective-permute-done((bf16[128,2048]{1,0:T(8,128)(2,1)S(1)}, bf16[128,2048]{1,0:T(8,128)(2,1)S(1)}, u32[]{:S(2)}, u32[]{:S(2)}) %collective-permute-start.3) | collective-permute-done | bytes 524320 | tf_op jit(solution)/shard_map/ppermute | solution.py:15
  84.6 5.2 collective-permute-start.4
  89.8 1.9 constant_dynamic-update-slice_fusion.15
  91.7 19.7 %collective-permute-done.4 = bf16[128,2048]{1,0:T(8,128)(2,1)S(1)} collective-permute-done((bf16[128,2048]{1,0:T(8,128)(2,1)S(1)}, bf16[128,2048]{1,0:T(8,128)(2,1)S(1)}, u32[]{:S(2)}, u32[]{:S(2)}) %collective-permute-start.4) | collective-permute-done | bytes 524320 | tf_op jit(solution)/shard_map/ppermute | solution.py:15
  111.4 5.2 collective-permute-start.5
  116.6 0.8 constant_dynamic-update-slice_fusion.14
  117.4 0.8 constant_dynamic-update-slice_fusion.13
  118.2 0.8 constant_dynamic-update-slice_fusion.12
  119.1 19.2 %collective-permute-done.5 = bf16[128,2048]{1,0:T(8,128)(2,1)S(1)} collective-permute-done((bf16[128,2048]{1,0:T(8,128)(2,1)S(1)}, bf16[128,2048]{1,0:T(8,128)(2,1)S(1)}, u32[]{:S(2)}, u32[]{:S(2)}) %collective-permute-start.5) | collective-permute-done | bytes 524320 | tf_op jit(solution)/shard_map/ppermute | solution.py:15
  138.3 5.2 collective-permute-start.6
  143.5 0.8 constant_dynamic-update-slice_fusion.11
  144.3 0.8 constant_dynamic-update-slice_fusion.10
  145.2 0.9 constant_dynamic-update-slice_fusion.9
  146.0 10.1 %collective-permute-done.6 = bf16[128,2048]{1,0:T(8,128)(2,1)S(1)} collective-permute-done((bf16[128,2048]{1,0:T(8,128)(2,1)S(1)}, bf16[128,2048]{1,0:T(8,128)(2,1)S(1)}, u32[]{:S(2)}, u32[]{:S(2)}) %collective-permute-start.6) | collective-permute-done | bytes 524320 | tf_op jit(solution)/shard_map/ppermute | solution.py:15
  156.1 0.8 constant_dynamic-update-slice_fusion.8
  157.0 0.8 constant_dynamic-update-slice_fusion.7
  157.8 0.8 constant_dynamic-update-slice_fusion.6
  158.7 0.9 constant_dynamic-update-slice_fusion.5
  159.5 0.8 constant_dynamic-update-slice_fusion.4
  160.3 0.8 constant_dynamic-update-slice_fusion.3
  161.2 0.8 constant_dynamic-update-slice_fusion.2
  162.0 0.8 constant_dynamic-update-slice_fusion.1
  162.8 0.9 constant_dynamic-update-slice_fusion
  163.7 6.8 %fusion.3 = f32[2048,512]{1,0:T(8,128)} fusion(bf16[512,1024]{1,0:T(8,128)(2,1)} %all-gather.4.cloned.1.call-done, bf16[2048,2048]{1,0:T(8,128)(2,1)} %constant_dynamic-update-slice_fusion, s32[]{:T(128)S(6)} %select_n.14), kind=kOutput, calls=%fused_computation.8 | convolution fusion | flops 2147483648 | bytes 9437188 | tf_op jit(solution)/shard_map/dot_general | solution.py:48
  170.5 8.1 %multiply_bitcast_fusion = f32[1024,2048]{0,1:T(8,128)} fusion(bf16[512,1024]{1,0:T(8,128)(2,1)} %all-gather.6.cloned.1.call-done, f32[2048,512]{1,0:T(8,128)} %fusion.3), kind=kOutput, calls=%fused_computation.1 | convolution fusion | flops 2152726528 | bytes 13631488 | tf_op jit(solution)/shard_map/dot_general | solution.py:32
  178.7 6.0 %fusion = bf16[512,2048]{0,1:T(8,128)(2,1)S(1)} fusion(f32[2048,512]{1,0:T(8,128)} %fusion.3, bf16[512,1024]{1,0:T(8,128)(2,1)S(1)} %copy-done.2, bf16[2048,1024]{1,0:T(8,128)(2,1)} %all-gather.8.cloned.1.call-done), kind=kOutput, calls=%fused_computation.4 | convolution fusion | flops 2151677952 | bytes 11534336 | tf_op jit(solution)/shard_map/dot_general | solution.py:32
  184.7 1.3 copy-done.4
  186.1 2.4 multiply_bitcast_fusion.1
  188.5 1.0 copy-done
  189.4 6.4 %pad_maximum_fusion = f32[1024,4096]{0,1:T(8,128)} fusion(f32[1024,2048]{0,1:T(8,128)S(1)} %copy-done, f32[1024,2048]{0,1:T(8,128)S(1)} %multiply_bitcast_fusion.1), kind=kLoop, calls=%fused_computation | loop fusion | flops 4194304 | bytes 33554432 | tf_op jit(solution)/shard_map/concatenate | solution.py:75
  196.1 1.3 copy-done.5
  197.4 5.9 fusion.1
  203.4 275.0 %reduce-scatter.5.cloned.1.call-done = f32[128,4096]{0,1:T(8,128)} async-done(((f32[1024,4096]{0,1:T(8,128)}), f32[128,4096]{0,1:T(8,128)}) %reduce-scatter.5.cloned.1.call-update) | async-done | bytes 2097168 | tf_op jit(solution)/shard_map/reduce_scatter | solution.py:28
  478.4 11.0 %reduce-scatter.3.cloned.1.call-done = f32[256,1024]{1,0:T(8,128)} async-done(((f32[512,1024]{1,0:T(8,128)}), f32[256,1024]{1,0:T(8,128)}) %reduce-scatter.3.cloned.1.call-update) | async-done | bytes 1048592 | tf_op jit(solution)/shard_map/reduce_scatter | solution.py:28
  489.4 2.1 convert_element_type.11
  491.4 64.3 %all-reduce.2.cloned.1.call-done = f32[128,4096]{0,1:T(8,128)} async-done(((f32[128,4096]{0,1:T(8,128)}), f32[128,4096]{0,1:T(8,128)}) %all-reduce.2.cloned.1.call-update) | async-done | bytes 2097168 | tf_op jit(solution)/shard_map/psum | solution.py:78
  555.8 2.4 multiply_reduce_fusion
  558.2 21.7 %psum.23 = f32[2048]{0:T(1024)S(1)} all-reduce(f32[2048]{0:T(1024)S(1)} %get-tuple-element.10), channel_id=1, replica_groups=mesh['rep'=2,'fs'=8,'tp'=2] {'fs'}, use_global_device_ids=true, to_apply=%region_6.7 | all-reduce | flops 2048 | bytes 16384 | tf_op jit(solution)/shard_map/psum | solution.py:83
  580.5 1.5 multiply_reduce_fusion.1
  582.0 2.5 psum.22
  584.9 1.3 copy.10
  (26 shorter events, 3.7 us)
Async XLA Ops:
  7.2 149.8 %copy-start.1 = (bf16[128,2048]{1,0:T(8,128)(2,1)S(1)}, bf16[128,2048]{1,0:T(8,128)(2,1)}, u32[]{:S(2)}) copy-start(bf16[128,2048]{1,0:T(8,128)(2,1)} %param.5) | copy-start | bytes 1572868
  7.2 156.6 %all-gather.4.cloned.1.call-start = ((), (), s32[]{:S(2)}) async-start(), calls=%async_computation.2 | async-start | bytes 1572864 | tf_op jit(solution)/shard_map/all_gather | solution.py:42
  7.9 162.6 %all-gather.6.cloned.1.call-start = ((), (), s32[]{:S(2)}) async-start(), calls=%async_computation.3 | async-start | bytes 1572864 | tf_op jit(solution)/shard_map/all_gather | solution.py:43
  8.7 170.0 %all-gather.8.cloned.1.call-start = ((), (), s32[]{:S(2)}) async-start(), calls=%async_computation.4 | async-start | bytes 4718592 | tf_op jit(solution)/shard_map/all_gather | solution.py:22
  9.4 469.0 %reduce-scatter.5.cloned.1.call-start = ((), (), s32[]{:S(2)}) async-start(), calls=%async_computation.6 | async-start | bytes 18874368 | tf_op jit(solution)/shard_map/reduce_scatter | solution.py:28
  9.4 17.6 %collective-permute-start = (bf16[128,2048]{1,0:T(8,128)(2,1)}, bf16[128,2048]{1,0:T(8,128)(2,1)S(1)}, u32[]{:S(2)}, u32[]{:S(2)}) collective-permute-start(bf16[128,2048]{1,0:T(8,128)(2,1)} %param.5), channel_id=1, source_target_pairs={{0,14},{2,0},{4,2},{6,4},{8,6},{10,8},{12,10},{14,12},{1,15},{3,1}... | collective-permute-start | bytes 1572872 | tf_op jit(solution)/shard_map/ppermute | solution.py:15
  27.0 15.4 %collective-permute-start.1 = (bf16[128,2048]{1,0:T(8,128)(2,1)S(1)}, bf16[128,2048]{1,0:T(8,128)(2,1)S(1)}, u32[]{:S(2)}, u32[]{:S(2)}) collective-permute-start(bf16[128,2048]{1,0:T(8,128)(2,1)S(1)} %collective-permute-done), channel_id=1, source_target_pairs={{0,14},{2,0},{4,2},{6,4},{8,6},{10,8},{12,10},{14,12},{1,15},{3,1}... | collective-permute-start | bytes 1572872 | tf_op jit(solution)/shard_map/ppermute | solution.py:15
  42.4 24.1 %collective-permute-start.2 = (bf16[128,2048]{1,0:T(8,128)(2,1)S(1)}, bf16[128,2048]{1,0:T(8,128)(2,1)S(1)}, u32[]{:S(2)}, u32[]{:S(2)}) collective-permute-start(bf16[128,2048]{1,0:T(8,128)(2,1)S(1)} %collective-permute-done.1), channel_id=1, source_target_pairs={{0,14},{2,0},{4,2},{6,4},{8,6},{10,8},{12,10},{14,12},{1,15},{3,1}... | collective-permute-start | bytes 1572872 | tf_op jit(solution)/shard_map/ppermute | solution.py:15
  66.6 18.0 %collective-permute-start.3 = (bf16[128,2048]{1,0:T(8,128)(2,1)S(1)}, bf16[128,2048]{1,0:T(8,128)(2,1)S(1)}, u32[]{:S(2)}, u32[]{:S(2)}) collective-permute-start(bf16[128,2048]{1,0:T(8,128)(2,1)S(1)} %collective-permute-done.2), channel_id=1, source_target_pairs={{0,14},{2,0},{4,2},{6,4},{8,6},{10,8},{12,10},{14,12},{1,15},{3,1}... | collective-permute-start | bytes 1572872 | tf_op jit(solution)/shard_map/ppermute | solution.py:15
  84.6 26.8 %collective-permute-start.4 = (bf16[128,2048]{1,0:T(8,128)(2,1)S(1)}, bf16[128,2048]{1,0:T(8,128)(2,1)S(1)}, u32[]{:S(2)}, u32[]{:S(2)}) collective-permute-start(bf16[128,2048]{1,0:T(8,128)(2,1)S(1)} %collective-permute-done.3), channel_id=1, source_target_pairs={{0,14},{2,0},{4,2},{6,4},{8,6},{10,8},{12,10},{14,12},{1,15},{3,1}... | collective-permute-start | bytes 1572872 | tf_op jit(solution)/shard_map/ppermute | solution.py:15
  111.4 26.9 %collective-permute-start.5 = (bf16[128,2048]{1,0:T(8,128)(2,1)S(1)}, bf16[128,2048]{1,0:T(8,128)(2,1)S(1)}, u32[]{:S(2)}, u32[]{:S(2)}) collective-permute-start(bf16[128,2048]{1,0:T(8,128)(2,1)S(1)} %collective-permute-done.4), channel_id=1, source_target_pairs={{0,14},{2,0},{4,2},{6,4},{8,6},{10,8},{12,10},{14,12},{1,15},{3,1}... | collective-permute-start | bytes 1572872 | tf_op jit(solution)/shard_map/ppermute | solution.py:15
  138.3 17.8 %collective-permute-start.6 = (bf16[128,2048]{1,0:T(8,128)(2,1)S(1)}, bf16[128,2048]{1,0:T(8,128)(2,1)S(1)}, u32[]{:S(2)}, u32[]{:S(2)}) collective-permute-start(bf16[128,2048]{1,0:T(8,128)(2,1)S(1)} %collective-permute-done.5), channel_id=1, source_target_pairs={{0,14},{2,0},{4,2},{6,4},{8,6},{10,8},{12,10},{14,12},{1,15},{3,1}... | collective-permute-start | bytes 1572872 | tf_op jit(solution)/shard_map/ppermute | solution.py:15
  170.5 8.1 %copy-start.2 = (bf16[512,1024]{1,0:T(8,128)(2,1)S(1)}, bf16[512,1024]{1,0:T(8,128)(2,1)}, u32[]{:S(2)}) copy-start(bf16[512,1024]{1,0:T(8,128)(2,1)} %all-gather.6.cloned.1.call-done) | copy-start | bytes 3145732
  178.7 7.4 %copy-start.3 = (bf16[512,1024]{1,0:T(8,128)(2,1)S(1)}, bf16[512,1024]{1,0:T(8,128)(2,1)}, u32[]{:S(2)}) copy-start(bf16[512,1024]{1,0:T(8,128)(2,1)} %all-gather.4.cloned.1.call-done) | copy-start | bytes 3145732
  184.7 1.3 copy-start.4
  186.1 3.4 copy-start
  195.8 1.6 copy-start.5
  195.8 293.5 %reduce-scatter.3.cloned.1.call-start = ((), (), s32[]{:S(2)}) async-start(), calls=%async_computation.5 | async-start | bytes 3145728 | tf_op jit(solution)/shard_map/reduce_scatter | solution.py:28
  203.3 352.5 %all-reduce.2.cloned.1.call-start = ((), (), s32[]{:S(2)}) async-start(), calls=%async_computation.7 | async-start | bytes 4194304 | tf_op jit(solution)/shard_map/psum | solution.py:78
Sparse Core Ops, SparseCore 0:
  9.5 11.7 all-gather.3
  22.9 10.1 all-gather.5
  35.1 114.6 all-gather.7
  196.0 282.3 reduce-scatter.4
  480.5 8.8 reduce-scatter.2
  491.5 64.2 all-reduce.1
